TPU v7x, 32 devices: a whole 2x2x4 slice. The times are simulated.
32 devices in a mesh: ep: 8 (over z, y), tp: 4 (over x, core).
Axes of the slice: x: 2, y: 2, z: 4, core: 2. Of those that a mesh axis runs over, the one named last changes fastest.
Arguments:
- tokens: bfloat16 [24, 2048], P('ep'), may hold values from -6 to 6
- pre_gain: float32 [2048], replicated, may hold values from 0.1 to 1.9
- w_query: bfloat16 [2048, 2048], P('tp', 'ep'), may hold values from -0.125 to 0.125
- w_forget: bfloat16 [2048, 2048], P('tp', 'ep'), may hold values from -0.125 to 0.125
- w_input: bfloat16 [2048, 2048], P('tp', 'ep'), may hold values from -0.125 to 0.125
- w_outgate: bfloat16 [2048, 2048], P('tp', 'ep'), may hold values from -0.125 to 0.125
- lower_bound: float32 [2048], P('tp'), may hold values from 0 to 0.9
- head_gain: float32 [2048], P('tp'), may hold values from 0.1 to 1.9
- w_output: bfloat16 [2048, 2048], P('tp', 'ep'), may hold values from -0.125 to 0.125
- mix_gain: float32 [2048], replicated, may hold values from 0.1 to 1.9
- ffn_gain: float32 [2048], replicated, may hold values from 0.1 to 1.9
- post_gain: float32 [2048], replicated, may hold values from 0.1 to 1.9
- state: float32 [24, 16, 128, 128], P('ep', 'tp'), may hold values from -4 to 4
- routes: int32 [24, 2], P('ep'), may hold values from 0 to 7, all different within a row; in each aligned block of 24 rows (0 to 23, 24 to 47, ...) at most 12 rows name the same one
- route_scores: float32 [24, 2], P('ep'), may hold values from 0.1 to 1
- w_gate: bfloat16 [8, 2048, 512], P('ep', None, 'tp'), may hold values from -0.125 to 0.125
- w_up: bfloat16 [8, 2048, 512], P('ep', None, 'tp'), may hold values from -0.125 to 0.125
- w_down: bfloat16 [8, 512, 2048], P('ep', 'tp'), may hold values from -0.25 to 0.25
Outputs:
- layer_out: bfloat16 [24, 2048], P('ep')
- new_state: float32 [24, 16, 128, 128], P('ep', 'tp')
Inputs may be any that keep to these rules, and one draw needn't show every extreme that they name: `routes`: over all 24 tokens no expert is named more than 12 times, a bound that some block reaches; a row never names one expert twice.
All inputs are finite; a program needn't handle non-finite values.
Results may differ from a plain program's by a relative error of at most 0.023.
Values may be sent and summed in bfloat16 or wider, within the bound.
A program may use at most 64 MiB of HBM per device.

v0:
```python
import jax
import jax.numpy as jnp
from jax import lax
from jax.sharding import PartitionSpec as P

CAP = 12


EPSILON = 1e-06


def rms_scale(values, gain):
    floats = values.astype(jnp.float32)
    return floats * lax.rsqrt(jnp.mean(floats * floats, axis=-1, keepdims=True) + EPSILON) * gain


def per_device(
    tokens,
    pre_gain,
    w_query,
    w_forget,
    w_input,
    w_outgate,
    lower_bound,
    head_gain,
    w_output,
    mix_gain,
    ffn_gain,
    post_gain,
    state,
    routes,
    route_scores,
    w_gate,
    w_up,
    w_down,
):
    row_count, model_width = tokens.shape
    tp_count = lax.axis_size("tp")
    quarter = model_width // tp_count
    tp_index = lax.axis_index("tp")
    ep_index = lax.axis_index("ep")
    heads_here = state.shape[1]
    head_size = state.shape[2]
    normed = rms_scale(tokens, pre_gain).astype(jnp.bfloat16)
    own_block = lax.dynamic_slice_in_dim(normed, tp_index * quarter, quarter, 1)
    block_rows = lax.all_gather(own_block, "ep", axis=0, tiled=True)
    partial_in = jnp.stack(
        [
            jnp.dot(block_rows, weight, preferred_element_type=jnp.float32)
            for weight in (w_query, w_forget, w_input, w_outgate)
        ],
        axis=1,
    ).astype(jnp.bfloat16)
    by_token = lax.all_to_all(partial_in, "ep", split_axis=0, concat_axis=2, tiled=True)
    summed = lax.psum_scatter(
        by_token.astype(jnp.float32).astype(jnp.bfloat16), "tp", scatter_dimension=2, tiled=True
    )
    query_pre = summed[:, 0]
    forget_pre = summed[:, 1]
    input_pre = summed[:, 2]
    gate_pre = summed[:, 3]
    shaped = (row_count, heads_here, head_size)
    forget = lower_bound + (1.0 - lower_bound) * jax.nn.sigmoid(forget_pre.astype(jnp.float32))
    queries = jax.nn.silu(query_pre.astype(jnp.float32))
    new_state = (
        forget.reshape(shaped)[..., None] * state
        + (1.0 - forget).reshape(shaped)[..., None]
        * input_pre.astype(jnp.float32).reshape(shaped)[..., None, :]
    )
    readout = jnp.einsum("shk,shkv->shv", queries.reshape(shaped), new_state)
    readout = readout * lax.rsqrt(jnp.mean(readout * readout, axis=-1, keepdims=True) + EPSILON)
    readout = readout * head_gain.reshape(heads_here, head_size)
    gated_out = (
        readout.reshape(row_count, quarter) * jax.nn.silu(gate_pre.astype(jnp.float32))
    ).astype(jnp.bfloat16)
    partial_out = jnp.dot(
        lax.all_gather(gated_out, "ep", axis=0, tiled=True),
        w_output,
        preferred_element_type=jnp.float32,
    ).astype(jnp.bfloat16)
    out_token = lax.all_to_all(partial_out, "ep", split_axis=0, concat_axis=1, tiled=True)
    mixer_out = lax.psum(out_token.astype(jnp.float32).astype(jnp.bfloat16), "tp")
    residual = (tokens.astype(jnp.float32) + rms_scale(mixer_out, mix_gain)).astype(jnp.bfloat16)
    ffn_in = rms_scale(residual, ffn_gain).astype(jnp.bfloat16)
    route_count = routes.shape[1]
    exp_dev = w_gate.shape[0]
    capacity = CAP
    weights = route_scores / jnp.sum(route_scores, axis=-1, keepdims=True)
    all_routes, all_weights = (
        lax.all_gather(routes.astype(jnp.float32), "ep", axis=0, tiled=True),
        lax.all_gather(weights, "ep", axis=0, tiled=True),
    )
    all_rows = lax.all_gather(ffn_in, "ep", axis=0, tiled=True)
    seq_total = all_rows.shape[0]
    flat_routes = all_routes.astype(jnp.int32).reshape(-1)
    own_ids = ep_index * exp_dev + jnp.arange(exp_dev, dtype=jnp.int32)
    mine = flat_routes[None, :] == own_ids[:, None]
    rank = jnp.cumsum(mine.astype(jnp.int32), axis=1) - 1
    slot_ids = jnp.arange(capacity, dtype=jnp.int32)
    matched = jnp.logical_and(mine[:, None, :], rank[:, None, :] == slot_ids[None, :, None])
    matched = matched.astype(jnp.float32).reshape(exp_dev, capacity, seq_total, route_count)
    placing = jnp.sum(matched, axis=3).astype(jnp.bfloat16)
    selected = jnp.einsum(
        "ecs,sd->ecd", placing, all_rows, preferred_element_type=jnp.float32
    ).astype(jnp.bfloat16)
    gate_val = jnp.einsum("ecd,edf->ecf", selected, w_gate, preferred_element_type=jnp.float32)
    up_val = jnp.einsum("ecd,edf->ecf", selected, w_up, preferred_element_type=jnp.float32)
    hidden = (jax.nn.silu(gate_val) * up_val).astype(jnp.bfloat16)
    partial_value = jnp.einsum(
        "ecf,efd->ecd", hidden, w_down, preferred_element_type=jnp.float32
    ).astype(jnp.bfloat16)
    reduced = lax.psum_scatter(
        partial_value.astype(jnp.float32).astype(jnp.bfloat16),
        "tp",
        scatter_dimension=2,
        tiled=True,
    )
    every_expert = lax.all_gather(reduced, "ep", axis=0, tiled=True)
    slot_rows = every_expert.reshape(-1, reduced.shape[2])
    own_flat = routes.reshape(-1)
    flat_count = own_flat.shape[0]
    own_pos = ep_index * flat_count + jnp.arange(flat_count, dtype=jnp.int32)
    all_pos = jnp.arange(flat_routes.shape[0], dtype=jnp.int32)
    earlier = jnp.logical_and(
        flat_routes[None, :] == own_flat[:, None], all_pos[None, :] < own_pos[:, None]
    )
    own_rank = jnp.sum(earlier.astype(jnp.int32), axis=1)
    picked = slot_rows[own_flat * capacity + own_rank].astype(jnp.float32)
    picked = picked.reshape(row_count, route_count, -1)
    combined_block = jnp.sum(picked * weights[..., None], axis=1)
    combined = lax.all_gather(combined_block, "tp", axis=1, tiled=True)
    layer_out = (residual.astype(jnp.float32) + rms_scale(combined, post_gain)).astype(jnp.bfloat16)
    return (layer_out, new_state)


def solution(mesh):
    in_specs = (
        P("ep", None),
        P(),
        P("tp", "ep"),
        P("tp", "ep"),
        P("tp", "ep"),
        P("tp", "ep"),
        P("tp"),
        P("tp"),
        P("tp", "ep"),
        P(),
        P(),
        P(),
        P("ep", "tp", None, None),
        P("ep", None),
        P("ep", None),
        P("ep", None, "tp"),
        P("ep", None, "tp"),
        P("ep", "tp", None),
    )
    out_specs = (P("ep", None), P("ep", "tp", None, None))
    return jax.shard_map(
        per_device, mesh=mesh, in_specs=in_specs, out_specs=out_specs, check_vma=False
    )
```

profile of v0, /device:TPU:0, one launch (start us, length us, event | category | flops | bytes accessed | tf_op | source)
XLA Modules:
  0.0 257.5 jit_solution(13783654858924082019)
XLA Ops:
  7.2 0.8 convert_element_type.133
  8.0 0.8 multiply_reduce_fusion.1
  8.8 0.8 dynamic-slice
  9.7 32.4 %all-gather = bf16[8,3,512]{2,1,0:T(4,128)(2,1)S(1)} all-gather(bf16[1,3,512]{2,1,0:T(4,128)(2,1)S(1)} %fusion.32), channel_id=1, replica_groups=mesh['ep'=8,'tp'=4] {'ep'}, dimensions={0}, use_global_device_ids=true | all-gather | bytes 27648 | tf_op jit(solution)/shard_map/all_gather | solution.py:46
  42.1 1.1 fusion.1
  43.2 1.1 fusion.2
  44.3 1.1 fusion.3
  45.4 1.1 fusion.4
  46.5 0.6 copy.63
  47.2 5.5 %all-to-all-start = ((bf16[24,4,256]{2,1,0:T(4,128)(2,1)}), bf16[24,4,256]{2,1,0:T(4,128)(2,1)S(1)}, u32[]{:S(2)}, u32[]{:S(2)}) async-start(bf16[24,4,256]{2,1,0:T(4,128)(2,1)} %copy.63), calls=%async_computation | async-start | bytes 98304 | tf_op jit(solution)/shard_map/all_to_all | solution.py:54
  52.7 0.8 broadcast_multiply_fusion
  53.5 0.8 copy.71
  54.2 0.7 subtract_bitcast_fusion
  54.9 20.9 %all-gather.2 = f32[8,3,2]{1,2,0:T(2,128)S(1)} all-gather(f32[1,3,2]{1,2,0:T(2,128)S(1)} %get-tuple-element.10), channel_id=1, replica_groups=mesh['ep'=8,'tp'=4] {'ep'}, dimensions={0}, use_global_device_ids=true | all-gather | bytes 216 | tf_op jit(solution)/shard_map/all_gather | solution.py:90
  75.9 0.1 copy.65
  76.0 0.1 copy.70
  76.1 0.1 eq.67
  76.2 0.1 eq.69
  76.3 0.1 copy.69
  76.4 0.1 mul.218
  76.5 0.7 reduce_sum.90
  77.2 0.7 broadcast_divide_fusion
  77.9 0.2 convert_reduce_fusion
  78.0 0.1 copy.66
  78.1 0.1 reshape.312
  78.3 0.1 copy.67
  78.3 0.1 reshape.291
  78.4 0.2 reduce_window_sum.11
  78.7 1.4 copy.77
  80.0 2.1 reshape.315
  82.2 0.1 sub.23
  82.3 18.8 %reduce-scatter.7.cloned.1.call-done = bf16[512,12]{1,0:T(8,128)(2,1)} async-done(((bf16[2048,12]{1,0:T(8,128)(2,1)}), bf16[512,12]{1,0:T(8,128)(2,1)}) %reduce-scatter.7.cloned.1.call-update) | async-done | bytes 12304
  101.2 1.4 reshape.316
  102.6 2.0 slice_convert_fusion.1
  104.6 0.6 add_divide_fusion
  105.2 1.6 copy.87
  106.8 0.3 copy.86
  107.1 1.5 copy.85
  108.7 0.5 multiply_add_fusion
  109.2 0.2 fusion.40
  109.4 0.1 multiply_reduce_fusion.3
  109.5 0.3 copy.88
  109.9 30.7 %all-gather.1 = bf16[8,3,512]{2,1,0:T(4,128)(2,1)S(1)} all-gather(bf16[1,3,512]{2,1,0:T(4,128)(2,1)S(1)} %fusion.36), channel_id=1, replica_groups=mesh['ep'=8,'tp'=4] {'ep'}, dimensions={0}, use_global_device_ids=true | all-gather | bytes 27648 | tf_op jit(solution)/shard_map/all_gather | solution.py:77
  140.6 1.1 convolution_convert_fusion.2
  141.7 0.6 all_to_all.31
  142.3 5.5 %all-to-all-start.1 = ((bf16[8,3,256]{2,1,0:T(4,128)(2,1)}), bf16[8,3,256]{2,1,0:T(4,128)(2,1)S(1)}, u32[]{:S(2)}, u32[]{:S(2)}) async-start(bf16[8,3,256]{2,1,0:T(4,128)(2,1)} %all_to_all.31), calls=%async_computation.1 | async-start | bytes 32768 | tf_op jit(solution)/shard_map/all_to_all | solution.py:81
  147.9 0.1 copy.72
  148.0 6.4 %all-to-all-done.1 = bf16[8,3,256]{2,1,0:T(4,128)(2,1)S(1)} async-done(((bf16[8,3,256]{2,1,0:T(4,128)(2,1)}), bf16[8,3,256]{2,1,0:T(4,128)(2,1)S(1)}, u32[]{:S(2)}, u32[]{:S(2)}) %all-to-all-start.1) | async-done | bytes 12320 | tf_op jit(solution)/shard_map/all_to_all | solution.py:81
  154.4 10.2 %psum.7 = bf16[3,2048]{1,0:T(4,128)(2,1)S(1)} all-reduce(bf16[3,2048]{1,0:T(4,128)(2,1)S(1)} %bitcast.99), channel_id=1, replica_groups=mesh['ep'=8,'tp'=4] {'tp'}, use_global_device_ids=true, to_apply=%region_3.4 | all-reduce | flops 6144 | bytes 24576 | tf_op jit(solution)/shard_map/psum | solution.py:82
  164.6 0.1 fusion.11
  164.8 0.2 fusion.15
  165.0 0.1 fusion.19
  165.1 30.5 %all-gather.3 = bf16[8,3,2048]{2,1,0:T(4,128)(2,1)S(1)} all-gather(bf16[1,3,2048]{2,1,0:T(4,128)(2,1)S(1)} %fusion.19), channel_id=1, replica_groups=mesh['ep'=8,'tp'=4] {'ep'}, dimensions={0}, use_global_device_ids=true | all-gather | bytes 110592 | tf_op jit(solution)/shard_map/all_gather | solution.py:93
  195.6 0.1 reshape.308
  195.7 0.1 convolution_convert_fusion.1
  195.8 0.2 fusion.9
  196.0 1.0 fusion
  197.1 16.1 %reduce-scatter.5.cloned.1.call-done = bf16[1,12,512]{2,1,0:T(8,128)(2,1)} async-done(((bf16[1,12,2048]{2,1,0:T(8,128)(2,1)}), bf16[1,12,512]{2,1,0:T(8,128)(2,1)}) %reduce-scatter.5.cloned.1.call-update) | async-done | bytes 12304 | tf_op jit(solution)/shard_map/reduce_scatter | solution.py:112
  213.1 30.8 %all_gather.22 = bf16[8,12,512]{2,1,0:T(8,128)(2,1)S(1)} all-gather(bf16[1,12,512]{2,1,0:T(8,128)(2,1)} %reduce-scatter.5.cloned.1.call-done), channel_id=1, replica_groups=mesh['ep'=8,'tp'=4] {'ep'}, dimensions={0}, use_global_device_ids=true | all-gather | bytes 110592 | tf_op jit(solution)/shard_map/all_gather | solution.py:118
  244.0 0.6 gather_fusion
  244.6 0.1 multiply_reduce_fusion.2
  244.6 5.2 %all_gather.23 = f32[3,2048]{1,0:T(4,128)S(1)} all-gather(f32[3,512]{1,0:T(4,128)S(1)} %multiply_reduce_fusion.2), channel_id=1, replica_groups=mesh['ep'=8,'tp'=4] {'tp'}, dimensions={1}, use_global_device_ids=true | all-gather | bytes 30720 | tf_op jit(solution)/shard_map/all_gather | solution.py:131
  249.8 0.1 multiply_reduce_fusion
  250.0 0.7 fusion.18
  (51 shorter events, 0.7 us)
Async XLA Ops:
  7.2 188.9 %copy-start = (bf16[1,128,2048]{2,1,0:T(8,128)(2,1)S(1)}, bf16[1,128,2048]{2,1,0:T(8,128)(2,1)}, u32[]{:S(2)}) copy-start(bf16[1,128,2048]{2,1,0:T(8,128)(2,1)} %param.35) | copy-start | bytes 1572868
  47.2 31.5 %all-to-all-start = ((bf16[24,4,256]{2,1,0:T(4,128)(2,1)}), bf16[24,4,256]{2,1,0:T(4,128)(2,1)S(1)}, u32[]{:S(2)}, u32[]{:S(2)}) async-start(bf16[24,4,256]{2,1,0:T(4,128)(2,1)} %copy.63), calls=%async_computation | async-start | bytes 98304 | tf_op jit(solution)/shard_map/all_to_all | solution.py:54
  52.7 48.5 %reduce-scatter.7.cloned.1.call-start = ((), (), s32[]{:S(2)}) async-start(), calls=%async_computation.5 | async-start | bytes 655360
  104.6 4.0 %copy-start.9 = (f32[512]{0:T(512)S(1)}, f32[512]{0:T(512)}, u32[]{:S(2)}) copy-start(f32[512]{0:T(512)} %param.24) | copy-start | bytes 6148
  105.2 3.4 %copy-start.2 = (f32[3,4,128,128]{3,2,1,0:T(8,128)S(1)}, f32[3,4,128,128]{3,2,1,0:T(8,128)}, u32[]{:S(2)}) copy-start(f32[3,4,128,128]{3,2,1,0:T(8,128)} %param.30) | copy-start | bytes 2359300
  107.1 2.7 %copy-start.10 = (f32[512]{0:T(512)S(1)}, f32[512]{0:T(512)}, u32[]{:S(2)}) copy-start(f32[512]{0:T(512)} %param.25) | copy-start | bytes 6148
  108.6 56.1 %copy-start.5 = (bf16[3,2048]{1,0:T(4,128)(2,1)S(1)}, bf16[3,2048]{1,0:T(4,128)(2,1)}, u32[]{:S(2)}) copy-start(bf16[3,2048]{1,0:T(4,128)(2,1)} %param.18) | copy-start | bytes 36868
  108.6 56.2 %copy-start.6 = (f32[2048]{0:T(1024)S(1)}, f32[2048]{0:T(1024)}, u32[]{:S(2)}) copy-start(f32[2048]{0:T(1024)} %param.27) | copy-start | bytes 24580
  108.6 56.4 %copy-start.8 = (f32[2048]{0:T(1024)S(1)}, f32[2048]{0:T(1024)}, u32[]{:S(2)}) copy-start(f32[2048]{0:T(1024)} %param.28) | copy-start | bytes 24580
  109.1 87.9 %copy-start.1 = (f32[3,4,128,128]{3,2,1,0:T(8,128)}, f32[3,4,128,128]{3,2,1,0:T(8,128)S(1)}, u32[]{:S(2)}) copy-start(f32[3,4,128,128]{3,2,1,0:T(8,128)S(1)} %multiply_add_fusion) | copy-start | bytes 2359300
  109.1 86.7 %copy-start.4 = (bf16[1,2048,128]{2,1,0:T(8,128)(2,1)S(1)}, bf16[1,2048,128]{2,1,0:T(8,128)(2,1)}, u32[]{:S(2)}) copy-start(bf16[1,2048,128]{2,1,0:T(8,128)(2,1)} %param.33) | copy-start | bytes 1572868
  109.2 86.9 %copy-start.3 = (bf16[1,2048,128]{2,1,0:T(8,128)(2,1)S(1)}, bf16[1,2048,128]{2,1,0:T(8,128)(2,1)}, u32[]{:S(2)}) copy-start(bf16[1,2048,128]{2,1,0:T(8,128)(2,1)} %param.34) | copy-start | bytes 1572868
  109.5 140.5 %copy-start.7 = (f32[2048]{0:T(1024)S(1)}, f32[2048]{0:T(1024)}, u32[]{:S(2)}) copy-start(f32[2048]{0:T(1024)} %param.29) | copy-start | bytes 24580
  142.3 12.1 %all-to-all-start.1 = ((bf16[8,3,256]{2,1,0:T(4,128)(2,1)}), bf16[8,3,256]{2,1,0:T(4,128)(2,1)S(1)}, u32[]{:S(2)}, u32[]{:S(2)}) async-start(bf16[8,3,256]{2,1,0:T(4,128)(2,1)} %all_to_all.31), calls=%async_computation.1 | async-start | bytes 32768 | tf_op jit(solution)/shard_map/all_to_all | solution.py:81
  147.8 65.3 %reduce-scatter.5.cloned.1.call-start = ((), (), s32[]{:S(2)}) async-start(), calls=%async_computation.4 | async-start | bytes 81920 | tf_op jit(solution)/shard_map/reduce_scatter | solution.py:112
Sparse Core Ops, SparseCore 0:
  82.3 18.8 reduce-scatter.6
  197.2 15.9 reduce-scatter.4
where the time goes:
time: 258 us
  blocking collectives  161 us (62%)
  waiting for transfers between devices  41.4 us (16%)
  between operations  14.3 us (6%)
  local copies, waits for them, and re-layouts  13.3 us (5%)
  starting transfers between devices  11 us (4%)
  other arithmetic  9.68 us (4%)
  matrix products  7.04 us (3%)
    all_gather x1, blocking collectives, per_device(): block_rows = lax.all_gather(own_block, 'ep', axis=0, tiled=True)  32.4 us
    all_gather x1, blocking collectives, per_device(): every_expert = lax.all_gather(reduced, 'ep', axis=0, tiled=True)  30.8 us
    all_gather x1, blocking collectives, per_device(): lax.all_gather(gated_out, 'ep', axis=0, tiled=True)  30.7 us
    all_gather x1, blocking collectives, per_device(): all_rows = lax.all_gather(ffn_in, 'ep', axis=0, tiled=True)  30.5 us
    all_gather x1, blocking collectives, per_device(): lax.all_gather(routes.astype(jnp.float32), 'ep', axis=0, tiled=True)  20.9 us
    unnamed x3, waiting for transfers between devices  18.9 us
    reduce_scatter x1, waiting for transfers between devices, per_device(): lax.psum_scatter(partial_value.astype(jnp.float32).astype(jnp.bfloat16),...  16.1 us
    psum x1, blocking collectives, per_device(): lax.psum(out_token.astype(jnp.float32).astype(jnp.bfloat16), 'tp')  10.2 us
  transfers between devices with their start and end apart: 4, of which 3 were waited for; matrix products, arithmetic and copies ran while one was open for 2% of the time, Pallas kernels for 0%

commit v1 on v0

--- a/solution.py
+++ b/solution.py
@@ -1,6 +1,10 @@
+import functools
+
 import jax
 import jax.numpy as jnp
 from jax import lax
+from jax.experimental import pallas as pl
+from jax.experimental.pallas import tpu as pltpu
 from jax.sharding import PartitionSpec as P
 
 CAP = 12
@@ -14,7 +18,7 @@
     return floats * lax.rsqrt(jnp.mean(floats * floats, axis=-1, keepdims=True) + EPSILON) * gain
 
 
-def per_device(
+def plain_device(
     tokens,
     pre_gain,
     w_query,
@@ -133,6 +137,427 @@
     return (layer_out, new_state)
 
 
+MESH = pl.DeviceIdType.MESH
+F32 = jnp.float32
+BF16 = jnp.bfloat16
+
+
+def silu(values):
+    return values / (1.0 + jnp.exp(-values))
+
+
+def rsqrt_mean(total, count):
+    return lax.rsqrt(total / count + EPSILON)
+
+
+def layer_kernel(
+    ep_n,
+    tp_n,
+    rows,
+    pad,
+    tokens_h, pre_gain_h, wq_h, wf_h, wi_h, wo_gate_h, lower_h, head_gain_h, w_out_h,
+    mix_gain_h, ffn_gain_h, post_gain_h, state_h, routes_h, scores_h, wg_h, wu_h, wd_h,
+    layer_ref, new_state_h,
+    tok, pre_gain, w_in, lower, head_gain, w_out, mix_gain, ffn_gain, post_gain, state,
+    routes, scores, wg, wu, wd,
+    tok_f, norm_send, tok_all, norm_all, dense_all, rows_f, tok_rows, dense_rows,
+    part_send, part_recv, fcol, qcol, read_rows, gate_all, gate_rows,
+    out_send, out_recv, mix_all, res_all, res_f,
+    exp_send, exp_recv, comb_all,
+    load_sem, store_sem,
+    s_norm, r_norm, s_tok, r_tok, s_dense, r_dense, s_part, r_part, s_gate, r_gate,
+    s_out, r_out, s_mix, r_mix, s_exp, r_exp, s_comb, r_comb,
+    barrier_unused,
+):
+    me_ep = lax.axis_index("ep")
+    me_tp = lax.axis_index("tp")
+    width = tok.shape[1]
+    quarter = width // tp_n
+    cols = w_out.shape[1]
+    per_tp = quarter // cols
+    heads, hsize = state.shape[1], state.shape[2]
+    all_n = ep_n * tp_n
+    me = me_ep * tp_n + me_tp
+    group = ep_n * pad // tp_n
+
+    loads = [
+        (tokens_h, tok), (pre_gain_h, pre_gain), (routes_h, routes), (scores_h, scores),
+        (wq_h, w_in.at[0]), (wf_h, w_in.at[1]), (wi_h, w_in.at[2]), (wo_gate_h, w_in.at[3]),
+        (lower_h, lower), (head_gain_h, head_gain), (state_h, state), (w_out_h, w_out),
+        (mix_gain_h, mix_gain), (ffn_gain_h, ffn_gain), (wg_h.at[0], wg), (wu_h.at[0], wu),
+        (wd_h.at[0], wd), (post_gain_h, post_gain),
+    ]
+    copies = [pltpu.make_async_copy(a, b, load_sem.at[k]) for k, (a, b) in enumerate(loads)]
+    for copy in copies:
+        copy.start()
+
+    barrier = pltpu.get_barrier_semaphore()
+
+    def greet(k, carry):
+        other = lax.rem(me + k, all_n)
+        pl.semaphore_signal(
+            barrier, inc=1, device_id={"ep": other // tp_n, "tp": lax.rem(other, tp_n)},
+            device_id_type=MESH,
+        )
+        return carry
+
+    lax.fori_loop(1, all_n, greet, 0)
+
+    tok_f[...] = jnp.zeros_like(tok_f)
+    dense_own = jnp.zeros((pad, hsize), F32)
+    rows_f[...] = jnp.zeros_like(rows_f)
+    for k in range(4):
+        copies[k].wait()
+    tok_f[0:rows, :] = tok[...].astype(F32)
+    toks = tok_f[...]
+    scale = rsqrt_mean(jnp.sum(toks * toks, axis=-1, keepdims=True), width)
+    normed = (toks * scale * pre_gain[...]).astype(BF16)
+    for q in range(tp_n):
+        norm_send[q] = normed[:, q * quarter : (q + 1) * quarter]
+    norm_all[me_ep] = norm_send[me_tp]
+    tok_all[me_ep] = toks.astype(BF16)
+    lane = lax.broadcasted_iota(jnp.int32, (rows, hsize), 1)
+    score = scores[...]
+    weight = score / jnp.sum(score, axis=-1, keepdims=True)
+    chosen = routes[...]
+    dense = jnp.zeros((rows, hsize), F32)
+    for r in range(chosen.shape[1]):
+        dense = jnp.where(lane == chosen[:, r : r + 1], weight[:, r : r + 1], dense)
+    dense_all[me_ep] = dense_own
+    dense_all[me_ep, 0:rows, :] = dense
+
+    pl.semaphore_wait(barrier, all_n - 1)
+
+    def to_ep(source, slot, send, recv, k):
+        return pltpu.make_async_remote_copy(
+            src_ref=source, dst_ref=slot, send_sem=send.at[k], recv_sem=recv.at[k],
+            device_id={"ep": lax.rem(me_ep + k, ep_n), "tp": me_tp}, device_id_type=MESH,
+        )
+
+    pending = []
+    norm_copies = [
+        to_ep(norm_send.at[me_tp], norm_all.at[me_ep], s_norm, r_norm, k) for k in range(1, ep_n)
+    ]
+    for copy in norm_copies:
+        copy.start()
+    side = [
+        to_ep(ref.at[me_ep], ref.at[me_ep], s, r, k)
+        for ref, s, r in ((tok_all, s_tok, r_tok), (dense_all, s_dense, r_dense))
+        for k in range(1, ep_n)
+    ]
+    for copy in side:
+        copy.start()
+    pending += norm_copies + side
+
+    for k in range(4, 8):
+        copies[k].wait()
+    for copy in norm_copies:
+        copy.wait_recv()
+    for i in range(ep_n):
+        rows_f[pl.ds(pad * i, pad), :] = norm_all[i].astype(F32)
+    x = rows_f[...].astype(BF16)
+    for m in range(4):
+        part = jnp.dot(x, w_in[m], preferred_element_type=F32)
+        for i in range(ep_n):
+            part_send[i, :, m * cols : (m + 1) * cols] = part[pad * i : pad * (i + 1)].astype(BF16)
+    home = me_ep // per_tp
+    slot = lax.rem(me_ep, per_tp) * tp_n + me_tp
+    for k in range(ep_n):
+        target = lax.rem(me_ep + k, ep_n)
+        copy = pltpu.make_async_remote_copy(
+            src_ref=part_send.at[target], dst_ref=part_recv.at[slot], send_sem=s_part.at[k],
+            recv_sem=r_part.at[slot], device_id={"ep": target, "tp": home}, device_id_type=MESH,
+        )
+        if k == 0:
+
+            @pl.when(home != me_tp)
+            def _():
+                copy.start()
+
+            @pl.when(home == me_tp)
+            def _():
+                part_recv[slot] = part_send[me_ep]
+
+            part_home = copy
+        else:
+            copy.start()
+            pending.append(copy)
+
+    for copy in side:
+        copy.wait_recv()
+    for i in range(ep_n):
+        tok_rows[pl.ds(pad * i, pad), :] = tok_all[i].astype(F32)
+        dense_rows[pl.ds(pad * i, pad), :] = dense_all[i]
+    for k in range(8, 11):
+        copies[k].wait()
+
+    for s in range(per_tp * tp_n):
+        source_ep = me_tp * per_tp + s // tp_n
+        source_tp = s % tp_n
+        local = jnp.logical_and(source_ep == me_ep, me_tp == source_tp)
+
+        @pl.when(jnp.logical_not(local))
+        def _():
+            pltpu.make_async_remote_copy(
+                src_ref=part_recv.at[s], dst_ref=part_recv.at[s], send_sem=s_part.at[0],
+                recv_sem=r_part.at[s], device_id={"ep": source_ep, "tp": source_tp},
+                device_id_type=MESH,
+            ).wait_recv()
+
+    sums = []
+    for b in range(per_tp):
+        total = part_recv[b * tp_n].astype(F32)
+        for t in range(1, tp_n):
+            total = total + part_recv[b * tp_n + t].astype(F32)
+        sums.append(total.astype(BF16).astype(F32))
+    query, forget, value, gate = [
+        jnp.concatenate([total[:, m * cols : (m + 1) * cols] for total in sums], axis=1)
+        for m in range(4)
+    ]
+    bound = lower[...]
+    forget = bound + (1.0 - bound) / (1.0 + jnp.exp(-forget))
+    query = silu(query)
+    for h in range(heads):
+        fcol[pl.ds(pad * h, pad), :] = forget[:, h * hsize : (h + 1) * hsize]
+        qcol[pl.ds(pad * h, pad), :] = query[:, h * hsize : (h + 1) * hsize]
+    forget_t = fcol[...].T
+    query_t = qcol[...].T
+    read_rows[...] = jnp.zeros_like(read_rows)
+    for s in range(rows):
+        for h in range(heads):
+            c = pad * h + s
+            f = forget_t[:, c : c + 1]
+            new = f * state[s, h] + (1.0 - f) * value[s : s + 1, h * hsize : (h + 1) * hsize]
+            state[s, h] = new
+            read_rows[c : c + 1, :] = jnp.sum(
+                query_t[:, c : c + 1] * new, axis=0, keepdims=True
+            )
+    readout = read_rows[...]
+    readout = readout * rsqrt_mean(jnp.sum(readout * readout, axis=-1, keepdims=True), hsize)
+    gated = jnp.concatenate([readout[pad * h : pad * (h + 1)] for h in range(heads)], axis=1)
+    gate_all[me_ep] = (gated * head_gain[...] * silu(gate)).astype(BF16)
+
+    gate_copies = [
+        to_ep(gate_all.at[me_ep], gate_all.at[me_ep], s_gate, r_gate, k) for k in range(1, ep_n)
+    ]
+    for copy in gate_copies:
+        copy.start()
+    pending += gate_copies
+    state_out = pltpu.make_async_copy(state, new_state_h, store_sem.at[0])
+    state_out.start()
+
+    copies[11].wait()
+    for copy in gate_copies:
+        copy.wait_recv()
+    for i in range(ep_n):
+        gate_rows[pl.ds(pad * i, pad), :] = gate_all[i].astype(F32)
+    part = jnp.dot(gate_rows[...].astype(BF16), w_out[...], preferred_element_type=F32)
+    for t in range(tp_n):
+        out_send[t] = part[group * t : group * (t + 1)].astype(BF16)
+
+    def to_tp(source, slot, send, recv, k):
+        return pltpu.make_async_remote_copy(
+            src_ref=source, dst_ref=slot, send_sem=send.at[k], recv_sem=recv.at[k],
+            device_id={"ep": me_ep, "tp": lax.rem(me_tp + k, tp_n)}, device_id_type=MESH,
+        )
+
+    out_copies = [
+        to_tp(out_send.at[lax.rem(me_tp + k, tp_n)], out_recv.at[me_tp], s_out, r_out, k)
+        for k in range(1, tp_n)
+    ]
+    for copy in out_copies:
+        copy.start()
+    pending += out_copies
+    out_recv[me_tp] = out_send[me_tp]
+    for copy in out_copies:
+        copy.wait_recv()
+    total = out_recv[0].astype(F32)
+    for t in range(1, tp_n):
+        total = total + out_recv[t].astype(F32)
+    mix_all[me] = total.astype(BF16)
+
+    def to_any(source, slot, send, recv, k):
+        other = lax.rem(me + k, all_n)
+        return pltpu.make_async_remote_copy(
+            src_ref=source, dst_ref=slot, send_sem=send.at[k], recv_sem=recv.at[k],
+            device_id={"ep": other // tp_n, "tp": lax.rem(other, tp_n)}, device_id_type=MESH,
+        )
+
+    def mix_copy(k):
+        return to_any(mix_all.at[me], mix_all.at[me], s_mix, r_mix, k)
+
+    lax.fori_loop(1, all_n, lambda k, c: (mix_copy(k).start(), c)[1], 0)
+    for k in range(12, 17):
+        copies[k].wait()
+    lax.fori_loop(1, all_n, lambda k, c: (mix_copy(k).wait_recv(), c)[1], 0)
+
+    mixed = jnp.concatenate(
+        [
+            jnp.concatenate([mix_all[j * tp_n + t].astype(F32) for t in range(tp_n)], axis=0)
+            for j in range(ep_n)
+        ],
+        axis=1,
+    )
+    scale = rsqrt_mean(jnp.sum(mixed * mixed, axis=-1, keepdims=True), width)
+    residual = (tok_rows[...] + mixed * scale * mix_gain[...]).astype(BF16).astype(F32)
+    res_f[...] = residual
+    scale = rsqrt_mean(jnp.sum(residual * residual, axis=-1, keepdims=True), width)
+    ffn_in = (residual * scale * ffn_gain[...]).astype(BF16)
+    for i in range(ep_n):
+        res_all[i] = residual[pad * i : pad * (i + 1)]
+
+    gate_val = jnp.dot(ffn_in, wg[...], preferred_element_type=F32)
+    up_val = jnp.dot(ffn_in, wu[...], preferred_element_type=F32)
+    hidden = (silu(gate_val) * up_val).astype(BF16)
+    all_dense = dense_rows[...]
+    lane = lax.broadcasted_iota(jnp.int32, all_dense.shape, 1)
+    own = jnp.sum(jnp.where(lane == me_ep, all_dense, 0.0), axis=-1, keepdims=True)
+    for t in range(tp_n):
+        piece = jnp.dot(
+            hidden, wd[:, t * quarter : (t + 1) * quarter], preferred_element_type=F32
+        )
+        piece = jnp.where(own > 0.0, piece * own, 0.0)
+        for i in range(ep_n):
+            exp_send[i * tp_n + t] = piece[pad * i : pad * (i + 1)].astype(BF16)
+
+    def exp_copy(k):
+        return to_any(
+            exp_send.at[lax.rem(me + k, all_n)], exp_recv.at[me], s_exp, r_exp, k
+        )
+
+    lax.fori_loop(1, all_n, lambda k, c: (exp_copy(k).start(), c)[1], 0)
+    exp_recv[me] = exp_send[me]
+    lax.fori_loop(1, all_n, lambda k, c: (exp_copy(k).wait_recv(), c)[1], 0)
+    total = exp_recv[0].astype(F32)
+    for k in range(1, all_n):
+        total = total + exp_recv[k].astype(F32)
+    comb_all[me_tp] = total
+    comb_copies = [
+        to_tp(comb_all.at[me_tp], comb_all.at[me_tp], s_comb, r_comb, k) for k in range(1, tp_n)
+    ]
+    for copy in comb_copies:
+        copy.start()
+    pending += comb_copies
+    copies[17].wait()
+    for copy in comb_copies:
+        copy.wait_recv()
+    combined = jnp.concatenate([comb_all[t] for t in range(tp_n)], axis=1)
+    scale = rsqrt_mean(jnp.sum(combined * combined, axis=-1, keepdims=True), width)
+    result = (res_all[me_ep] + combined * scale * post_gain[...]).astype(BF16)
+    layer_ref[...] = result[0:rows]
+
+    state_out.wait()
+    for copy in pending:
+        copy.wait_send()
+
+    @pl.when(home != me_tp)
+    def _():
+        part_home.wait_send()
+
+    lax.fori_loop(1, all_n, lambda k, c: (mix_copy(k).wait_send(), c)[1], 0)
+    lax.fori_loop(1, all_n, lambda k, c: (exp_copy(k).wait_send(), c)[1], 0)
+
+
+def fits(sizes, tokens, w_output, state, w_gate):
+    ep_n, tp_n = sizes["ep"], sizes["tp"]
+    pad = pl.next_power_of_2(max(tokens.shape[0], 4))
+    return (
+        w_gate.shape[0] == 1
+        and pad <= 8
+        and w_output.shape[1] % 128 == 0
+        and w_gate.shape[2] % 128 == 0
+        and state.shape[2] == 128
+        and ep_n <= state.shape[2]
+        and ep_n % tp_n == 0
+        and (ep_n * pad) % (8 * tp_n) == 0
+        and ep_n * tp_n <= 64
+    )
+
+
+def per_device(sizes, *args):
+    (
+        tokens, pre_gain, w_query, w_forget, w_input, w_outgate, lower_bound, head_gain,
+        w_output, mix_gain, ffn_gain, post_gain, state, routes, route_scores, w_gate, w_up,
+        w_down,
+    ) = args
+    if not fits(sizes, tokens, w_output, state, w_gate):
+        return plain_device(*args)
+    ep_n, tp_n = sizes["ep"], sizes["tp"]
+    rows, width = tokens.shape
+    pad = pl.next_power_of_2(max(rows, 4))
+    quarter = width // tp_n
+    cols = w_output.shape[1]
+    heads, hsize = state.shape[1], state.shape[2]
+    all_n = ep_n * tp_n
+    total = ep_n * pad
+    group = total // tp_n
+    hbm = pl.BlockSpec(memory_space=pl.ANY)
+    vmem = pltpu.VMEM
+    dma = pltpu.SemaphoreType.DMA
+    flat = [
+        tokens, pre_gain[None], w_query, w_forget, w_input, w_outgate, lower_bound[None],
+        head_gain[None], w_output, mix_gain[None], ffn_gain[None], post_gain[None], state,
+        routes, route_scores, w_gate, w_up, w_down,
+    ]
+    scratch = [
+        vmem((rows, width), BF16),
+        vmem((1, width), F32),
+        vmem((4,) + w_query.shape, BF16),
+        vmem((1, quarter), F32),
+        vmem((1, quarter), F32),
+        vmem(w_output.shape, BF16),
+        vmem((1, width), F32),
+        vmem((1, width), F32),
+        vmem((1, width), F32),
+        vmem(state.shape, F32),
+        vmem(routes.shape, jnp.int32),
+        vmem(route_scores.shape, F32),
+        vmem(w_gate.shape[1:], BF16),
+        vmem(w_up.shape[1:], BF16),
+        vmem(w_down.shape[1:], BF16),
+        vmem((pad, width), F32),
+        vmem((tp_n, pad, quarter), BF16),
+        vmem((ep_n, pad, width), BF16),
+        vmem((ep_n, pad, quarter), BF16),
+        vmem((ep_n, pad, hsize), F32),
+        vmem((total, quarter), F32),
+        vmem((total, width), F32),
+        vmem((total, hsize), F32),
+        vmem((ep_n, pad, 4 * cols), BF16),
+        vmem((ep_n, pad, 4 * cols), BF16),
+        vmem((heads * pad, hsize), F32),
+        vmem((heads * pad, hsize), F32),
+        vmem((heads * pad, hsize), F32),
+        vmem((ep_n, pad, quarter), BF16),
+        vmem((total, quarter), F32),
+        vmem((tp_n, group, cols), BF16),
+        vmem((tp_n, group, cols), BF16),
+        vmem((all_n, group, cols), BF16),
+        vmem((ep_n, pad, width), F32),
+        vmem((total, width), F32),
+        vmem((all_n, pad, quarter), BF16),
+        vmem((all_n, pad, quarter), BF16),
+        vmem((tp_n, pad, quarter), F32),
+        dma((18,)),
+        dma((1,)),
+    ]
+    for count in (ep_n, ep_n, ep_n, ep_n, ep_n, tp_n, all_n, all_n, tp_n):
+        scratch += [dma((count,)), dma((count,))]
+    scratch.append(pltpu.SemaphoreType.REGULAR)
+    return pl.pallas_call(
+        functools.partial(layer_kernel, ep_n, tp_n, rows, pad),
+        out_shape=(
+            jax.ShapeDtypeStruct(tokens.shape, BF16),
+            jax.ShapeDtypeStruct(state.shape, F32),
+        ),
+        in_specs=[hbm] * len(flat),
+        out_specs=(pl.BlockSpec(memory_space=pltpu.VMEM), hbm),
+        scratch_shapes=scratch,
+        compiler_params=pltpu.CompilerParams(collective_id=0, has_side_effects=True),
+        name="layer",
+    )(*flat)
+
+
 def solution(mesh):
     in_specs = (
         P("ep", None),
@@ -156,5 +581,5 @@
     )
     out_specs = (P("ep", None), P("ep", "tp", None, None))
     return jax.shard_map(
-        per_device, mesh=mesh, in_specs=in_specs, out_specs=out_specs, check_vma=False
-    )
+        functools.partial(per_device, mesh.shape), mesh=mesh, in_specs=in_specs, out_specs=out_specs, check_vma=False
+    )

time: 258 us -> 46.8 us (0.18)
  blocking collectives: 161 us -> 0 us
  waiting for transfers between devices: 41.4 us -> 0 us
  Pallas kernels: 0 us -> 40.4 us
  between operations: 14.3 us -> 0.65 us
  starting transfers between devices: 11 us -> 0 us
  other arithmetic: 9.68 us -> 0 us
  local copies, waits for them, and re-layouts: 13.3 us -> 5.4 us
  matrix products: 7.04 us -> 0 us
    all_gather x6 -> x0, blocking collectives: 151 us -> none  [the longest x1 32.4 us: per_device(): block_rows = lax.all_gather(own_block, 'ep', axis=0, tiled=True)]
    pallas_call x0 -> x1, Pallas kernels: none -> 40.4 us  [per_device(): pl.pallas_call(functools.partial(layer_kernel, ep_n, tp_n, rows, pad), ou...]
    unnamed x3 -> x0, waiting for transfers between devices: 18.9 us -> none
    reduce_scatter x1 -> x0, waiting for transfers between devices: 16.1 us -> none  [per_device(): lax.psum_scatter(partial_value.astype(jnp.float32).astype(jnp.bfloat16),...]
    all_to_all x2 -> x0, starting transfers between devices: 11 us -> none  [the longest x1 5.49 us: per_device(): lax.all_to_all(partial_in, 'ep', split_axis=0, concat_axis=2, tiled=True)]
    psum x1 -> x0, blocking collectives: 10.2 us -> none  [per_device(): lax.psum(out_token.astype(jnp.float32).astype(jnp.bfloat16), 'tp')]
    dot_general x9 -> x0, matrix products: 7.04 us -> none  [the longest x4 4.42 us: per_device(): jnp.dot(block_rows, weight, preferred_element_type=jnp.float32)]
    all_to_all x2 -> x0, waiting for transfers between devices: 6.4 us -> none  [the longest x1 6.4 us: per_device(): lax.all_to_all(partial_out, 'ep', split_axis=0, concat_axis=1, tiled=True)]
  transfers between devices with their start and end apart: 4 -> 0, of which waited for: 3 -> 0; matrix products, arithmetic and copies ran while one was open for 2% -> 0% of each run, Pallas kernels for 0% -> 0%
where the time goes in v1:
time: 46.8 us; the launch traced here: 46.4 us
  Pallas kernels  40.4 us (86%)
  local copies, waits for them, and re-layouts  5.4 us (12%)
  between operations  0.65 us (1%)
    pallas_call x1, Pallas kernels, per_device(): pl.pallas_call(functools.partial(layer_kernel, ep_n, tp_n, rows, pad), ou...  40.4 us
    unnamed x8, local copies, waits for them, and re-layouts  5.4 us

profile of v1, /device:TPU:0, one launch (start us, length us, event | category | flops | bytes accessed | tf_op | source)
XLA Modules:
  0.0 46.4 jit_solution(16776961270890114123)
XLA Ops:
  0.6 0.0 copy-start
  0.6 0.7 %copy-done = s32[3,2]{0,1:T(2,128)S(1)} copy-done((s32[3,2]{0,1:T(2,128)S(1)}, s32[3,2]{0,1:T(2,128)}, u32[]{:S(2)}) %copy-start) | copy-done | bytes 48
  1.3 0.0 copy-start.1
  1.3 0.7 %copy.20.routes_h = s32[3,2]{1,0:T(4,128)} copy(s32[3,2]{0,1:T(2,128)S(1)} %copy-done) | data formatting | bytes 48 | tf_op args[13]
  2.0 0.0 copy-done.1
  2.0 0.7 %copy.21.scores_h = f32[3,2]{1,0:T(4,128)} copy(f32[3,2]{0,1:T(2,128)S(1)} %copy-done.1) | data formatting | bytes 48 | tf_op args[14]
  2.7 40.4 %layer.1 = (bf16[3,2048]{1,0:T(4,128)(2,1)}, f32[3,4,128,128]{3,2,1,0:T(8,128)}) custom-call(bf16[3,2048]{1,0:T(4,128)(2,1)} %tokens_h.1, f32[1,2048]{1,0:T(1,128)} %bitcast.6, bf16[512,256]{1,0:T(8,128)(2,1)} %wq_h.1, bf16[512,256]{1,0:T(8,128)(2,1)} %wf_h.1, bf16[512,256]{1,0:T(8,128)(2,1)} %wi_h.1, bf16[512,256]{1,0:T(8,128)(2,1)} %wo_gate_h.1, ...), custom_call_target="tpu_custom_call" | custom-call | tf_op jit(solution)/shard_map/layer/pallas_call | solution.py:547
  43.0 1.3 %copy.24 = bf16[3,2048]{1,0:T(4,128)(2,1)} copy(bf16[3,2048]{1,0:T(4,128)(2,1)} %get-tuple-element.4) | data formatting | bytes 24576
  44.4 2.1 %copy.25 = f32[3,4,128,128]{3,2,1,0:T(8,128)} copy(f32[3,4,128,128]{3,2,1,0:T(8,128)} %get-tuple-element.5) | data formatting | bytes 1572864
Async XLA Ops:
  0.6 0.7 %copy-start = (s32[3,2]{0,1:T(2,128)S(1)}, s32[3,2]{0,1:T(2,128)}, u32[]{:S(2)}) copy-start(s32[3,2]{0,1:T(2,128)} %param.31) | copy-start | bytes 76
  1.3 0.7 %copy-start.1 = (f32[3,2]{0,1:T(2,128)S(1)}, f32[3,2]{0,1:T(2,128)}, u32[]{:S(2)}) copy-start(f32[3,2]{0,1:T(2,128)} %param.32) | copy-start | bytes 76

commit v2 on v1

--- a/solution.py
+++ b/solution.py
@@ -157,17 +157,16 @@
     pad,
     tokens_h, pre_gain_h, wq_h, wf_h, wi_h, wo_gate_h, lower_h, head_gain_h, w_out_h,
     mix_gain_h, ffn_gain_h, post_gain_h, state_h, routes_h, scores_h, wg_h, wu_h, wd_h,
-    layer_ref, new_state_h,
+    layer_ref, new_state,
     tok, pre_gain, w_in, lower, head_gain, w_out, mix_gain, ffn_gain, post_gain, state,
     routes, scores, wg, wu, wd,
-    tok_f, norm_send, tok_all, norm_all, dense_all, rows_f, tok_rows, dense_rows,
+    tok_f, dense_cols, norm_send, tok_all, norm_all, dense_all, rows_f, tok_rows, dense_rows,
     part_send, part_recv, fcol, qcol, read_rows, gate_all, gate_rows,
     out_send, out_recv, mix_all, res_all, res_f,
     exp_send, exp_recv, comb_all,
-    load_sem, store_sem,
+    load_sem,
     s_norm, r_norm, s_tok, r_tok, s_dense, r_dense, s_part, r_part, s_gate, r_gate,
     s_out, r_out, s_mix, r_mix, s_exp, r_exp, s_comb, r_comb,
-    barrier_unused,
 ):
     me_ep = lax.axis_index("ep")
     me_tp = lax.axis_index("tp")
@@ -193,20 +192,21 @@
 
     barrier = pltpu.get_barrier_semaphore()
 
-    def greet(k, carry):
-        other = lax.rem(me + k, all_n)
+    for k in range(1, ep_n):
         pl.semaphore_signal(
-            barrier, inc=1, device_id={"ep": other // tp_n, "tp": lax.rem(other, tp_n)},
+            barrier, inc=1, device_id={"ep": lax.rem(me_ep + k, ep_n), "tp": me_tp},
             device_id_type=MESH,
         )
-        return carry
-
-    lax.fori_loop(1, all_n, greet, 0)
+    for k in range(1, tp_n):
+        pl.semaphore_signal(
+            barrier, inc=1, device_id={"ep": me_ep, "tp": lax.rem(me_tp + k, tp_n)},
+            device_id_type=MESH,
+        )
 
     tok_f[...] = jnp.zeros_like(tok_f)
-    dense_own = jnp.zeros((pad, hsize), F32)
+    dense_cols[...] = jnp.zeros_like(dense_cols)
     rows_f[...] = jnp.zeros_like(rows_f)
-    for k in range(4):
+    for k in range(2):
         copies[k].wait()
     tok_f[0:rows, :] = tok[...].astype(F32)
     toks = tok_f[...]
@@ -216,17 +216,7 @@
         norm_send[q] = normed[:, q * quarter : (q + 1) * quarter]
     norm_all[me_ep] = norm_send[me_tp]
     tok_all[me_ep] = toks.astype(BF16)
-    lane = lax.broadcasted_iota(jnp.int32, (rows, hsize), 1)
-    score = scores[...]
-    weight = score / jnp.sum(score, axis=-1, keepdims=True)
-    chosen = routes[...]
-    dense = jnp.zeros((rows, hsize), F32)
-    for r in range(chosen.shape[1]):
-        dense = jnp.where(lane == chosen[:, r : r + 1], weight[:, r : r + 1], dense)
-    dense_all[me_ep] = dense_own
-    dense_all[me_ep, 0:rows, :] = dense
-
-    pl.semaphore_wait(barrier, all_n - 1)
+    pl.semaphore_wait(barrier, ep_n + tp_n - 2)
 
     def to_ep(source, slot, send, recv, k):
         return pltpu.make_async_remote_copy(
@@ -240,6 +230,17 @@
     ]
     for copy in norm_copies:
         copy.start()
+    for k in range(2, 4):
+        copies[k].wait()
+    expert = lax.broadcasted_iota(jnp.int32, (hsize, rows), 0)
+    score = scores[...]
+    weight = score / jnp.sum(score, axis=0, keepdims=True)
+    chosen = routes[...]
+    dense = jnp.zeros((hsize, rows), F32)
+    for r in range(chosen.shape[0]):
+        dense = jnp.where(expert == chosen[r : r + 1, :], weight[r : r + 1, :], dense)
+    dense_cols[:, 0:rows] = dense
+    dense_all[me_ep] = dense_cols[...].T[0:pad]
     side = [
         to_ep(ref.at[me_ep], ref.at[me_ep], s, r, k)
         for ref, s, r in ((tok_all, s_tok, r_tok), (dense_all, s_dense, r_dense))
@@ -328,7 +329,7 @@
             c = pad * h + s
             f = forget_t[:, c : c + 1]
             new = f * state[s, h] + (1.0 - f) * value[s : s + 1, h * hsize : (h + 1) * hsize]
-            state[s, h] = new
+            new_state[s, h] = new
             read_rows[c : c + 1, :] = jnp.sum(
                 query_t[:, c : c + 1] * new, axis=0, keepdims=True
             )
@@ -343,8 +344,6 @@
     for copy in gate_copies:
         copy.start()
     pending += gate_copies
-    state_out = pltpu.make_async_copy(state, new_state_h, store_sem.at[0])
-    state_out.start()
 
     copies[11].wait()
     for copy in gate_copies:
@@ -446,7 +445,6 @@
     result = (res_all[me_ep] + combined * scale * post_gain[...]).astype(BF16)
     layer_ref[...] = result[0:rows]
 
-    state_out.wait()
     for copy in pending:
         copy.wait_send()
 
@@ -456,6 +454,17 @@
 
     lax.fori_loop(1, all_n, lambda k, c: (mix_copy(k).wait_send(), c)[1], 0)
     lax.fori_loop(1, all_n, lambda k, c: (exp_copy(k).wait_send(), c)[1], 0)
+
+
+def store_kernel(layer, state, layer_h, state_h, sem):
+    copies = [
+        pltpu.make_async_copy(state, state_h, sem.at[0]),
+        pltpu.make_async_copy(layer, layer_h, sem.at[1]),
+    ]
+    for copy in copies:
+        copy.start()
+    for copy in copies:
+        copy.wait()
 
 
 def fits(sizes, tokens, w_output, state, w_gate):
@@ -491,13 +500,13 @@
     all_n = ep_n * tp_n
     total = ep_n * pad
     group = total // tp_n
-    hbm = pl.BlockSpec(memory_space=pl.ANY)
+    hbm = pl.BlockSpec(memory_space=pltpu.HBM)
     vmem = pltpu.VMEM
     dma = pltpu.SemaphoreType.DMA
     flat = [
         tokens, pre_gain[None], w_query, w_forget, w_input, w_outgate, lower_bound[None],
         head_gain[None], w_output, mix_gain[None], ffn_gain[None], post_gain[None], state,
-        routes, route_scores, w_gate, w_up, w_down,
+        routes.T, route_scores.T, w_gate, w_up, w_down,
     ]
     scratch = [
         vmem((rows, width), BF16),
@@ -510,12 +519,13 @@
         vmem((1, width), F32),
         vmem((1, width), F32),
         vmem(state.shape, F32),
-        vmem(routes.shape, jnp.int32),
-        vmem(route_scores.shape, F32),
+        vmem(routes.shape[::-1], jnp.int32),
+        vmem(route_scores.shape[::-1], F32),
         vmem(w_gate.shape[1:], BF16),
         vmem(w_up.shape[1:], BF16),
         vmem(w_down.shape[1:], BF16),
         vmem((pad, width), F32),
+        vmem((hsize, hsize), F32),
         vmem((tp_n, pad, quarter), BF16),
         vmem((ep_n, pad, width), BF16),
         vmem((ep_n, pad, quarter), BF16),
@@ -539,23 +549,33 @@
         vmem((all_n, pad, quarter), BF16),
         vmem((tp_n, pad, quarter), F32),
         dma((18,)),
-        dma((1,)),
     ]
     for count in (ep_n, ep_n, ep_n, ep_n, ep_n, tp_n, all_n, all_n, tp_n):
         scratch += [dma((count,)), dma((count,))]
-    scratch.append(pltpu.SemaphoreType.REGULAR)
-    return pl.pallas_call(
+    shapes = (
+        jax.ShapeDtypeStruct(tokens.shape, BF16),
+        jax.ShapeDtypeStruct(state.shape, F32),
+    )
+    held = pl.pallas_call(
         functools.partial(layer_kernel, ep_n, tp_n, rows, pad),
-        out_shape=(
-            jax.ShapeDtypeStruct(tokens.shape, BF16),
-            jax.ShapeDtypeStruct(state.shape, F32),
+        out_shape=(pltpu.VMEM(tokens.shape, BF16), pltpu.VMEM(state.shape, F32)),
+        in_specs=[hbm] * len(flat),
+        out_specs=(pl.BlockSpec(memory_space=pltpu.VMEM),) * 2,
+        scratch_shapes=scratch,
+        compiler_params=pltpu.CompilerParams(
+            collective_id=0, has_side_effects=True, vmem_limit_bytes=60 * 1024 * 1024
         ),
-        in_specs=[hbm] * len(flat),
-        out_specs=(pl.BlockSpec(memory_space=pltpu.VMEM), hbm),
-        scratch_shapes=scratch,
-        compiler_params=pltpu.CompilerParams(collective_id=0, has_side_effects=True),
         name="layer",
     )(*flat)
+    return pl.pallas_call(
+        store_kernel,
+        out_shape=shapes,
+        in_specs=[pl.BlockSpec(memory_space=pltpu.VMEM)] * 2,
+        out_specs=(hbm,) * 2,
+        scratch_shapes=[dma((2,))],
+        compiler_params=pltpu.CompilerParams(vmem_limit_bytes=4096 * 1024),
+        name="store",
+    )(*held)
 
 
 def solution(mesh):

time: 46.8 us -> 40.8 us (0.87)
  local copies, waits for them, and re-layouts: 5.4 us -> 0 us
  Pallas kernels: 40.4 us -> 39.9 us
    unnamed x8 -> x0, local copies, waits for them, and re-layouts: 5.4 us -> none
    pallas_call x1, Pallas kernels: 40.4 us -> 39 us  [per_device(): pl.pallas_call(functools.partial(layer_kernel, ep_n, tp_n, rows, pad), ou...]
    pallas_call x0 -> x1, Pallas kernels: none -> 0.9 us  [per_device(): pl.pallas_call(store_kernel, out_shape=shapes, in_specs=[pl.BlockSpec(mem...]
where the time goes in v2:
time: 40.8 us; the launch traced here: 40.5 us
  Pallas kernels  39.9 us (98%)
  between operations  0.65 us (2%)
    pallas_call x1, Pallas kernels, per_device(): pl.pallas_call(functools.partial(layer_kernel, ep_n, tp_n, rows, pad), ou...  39 us
    pallas_call x1, Pallas kernels, per_device(): pl.pallas_call(store_kernel, out_shape=shapes, in_specs=[pl.BlockSpec(mem...  0.9 us

profile of v2, /device:TPU:0, one launch (start us, length us, event | category | flops | bytes accessed | tf_op | source)
XLA Modules:
  0.0 40.5 jit_solution(17064914416881750354)
XLA Ops:
  0.6 39.0 %layer.1 = (bf16[3,2048]{1,0:T(4,128)(2,1)S(1)}, f32[3,4,128,128]{3,2,1,0:T(8,128)S(1)}) custom-call(bf16[3,2048]{1,0:T(4,128)(2,1)} %tokens_h.1, f32[1,2048]{1,0:T(1,128)} %bitcast.8, bf16[512,256]{1,0:T(8,128)(2,1)} %wq_h.1, bf16[512,256]{1,0:T(8,128)(2,1)} %wf_h.1, bf16[512,256]{1,0:T(8,128)(2,1)} %wi_h.1, bf16[512,256]{1,0:T(8,128)(2,1)} %wo_gate_h.1, ...), custom_call_target="tpu_custom_call" | custom-call | tf_op jit(solution)/shard_map/layer/pallas_call | solution.py:559
  39.6 0.9 %store.1 = (bf16[3,2048]{1,0:T(4,128)(2,1)}, f32[3,4,128,128]{3,2,1,0:T(8,128)}) custom-call(bf16[3,2048]{1,0:T(4,128)(2,1)S(1)} %get-tuple-element.4.layer, f32[3,4,128,128]{3,2,1,0:T(8,128)S(1)} %get-tuple-element.5.state), custom_call_target="tpu_custom_call" | custom-call | tf_op jit(solution)/shard_map/store/pallas_call | solution.py:570
